TPU v7x, 32 devices: a whole 2x2x4 slice. The times are simulated.
32 devices in a mesh: ep: 4 (over y, x), tp: 8 (over z, core).
Axes of the slice: x: 2, y: 2, z: 4, core: 2. Of those that a mesh axis runs over, the one named last changes fastest.
Arguments:
- hidden_in: bfloat16 [64, 4096], P('ep'), may hold values from -6 to 6
- attn_gain: float32 [4096], replicated, may hold values from 0.1 to 1.9
- query_weight: bfloat16 [4096, 4096], P('ep', 'tp'), may hold values from -0.09375 to 0.09375
- key_weight: bfloat16 [4096, 1024], P('ep', 'tp'), may hold values from -0.09375 to 0.09375
- value_weight: bfloat16 [4096, 1024], P('ep', 'tp'), may hold values from -0.09375 to 0.09375
- query_gain: float32 [128], replicated, may hold values from 0.1 to 1.9
- key_gain: float32 [128], replicated, may hold values from 0.1 to 1.9
- head_offset: float32 [32], P('tp'), may hold values from -7 to -2
- key_cache: bfloat16 [64, 1024, 1024], P('ep', None, 'tp'), may hold values from -6 to 6
- value_cache: bfloat16 [64, 1024, 1024], P('ep', None, 'tp'), may hold values from -6 to 6
- lengths: int32 [64], P('ep'), may hold values from 1 to 1024
- out_weight: bfloat16 [4096, 4096], P('tp', 'ep'), may hold values from -0.375 to 0.375
- expert_gain: float32 [4096], replicated, may hold values from 0.1 to 1.9
- routes: int32 [64, 2], P('ep'), may hold values from 0 to 3, all different within a row; in each aligned block of 16 rows (0 to 15, 16 to 31, ...) at most 16 rows name the same one
- route_weights: float32 [64, 2], P('ep'), may hold values from 0.1 to 1
- gate_weight: bfloat16 [4, 4096, 2048], P('ep', None, 'tp'), may hold values from -0.09375 to 0.09375
- up_weight: bfloat16 [4, 4096, 2048], P('ep', None, 'tp'), may hold values from -0.09375 to 0.09375
- down_weight: bfloat16 [4, 2048, 4096], P('ep', 'tp'), may hold values from -0.125 to 0.125
Outputs:
- layer_out: bfloat16 [64, 4096], P('ep', 'tp')
- fresh_keys: bfloat16 [64, 1024], P('ep', 'tp')
- fresh_values: bfloat16 [64, 1024], P('ep', 'tp')
Inputs may be any that keep to these rules, and one draw needn't show every extreme that they name: `routes`: each row names 2 different experts. Among the rows of one index of ep (16 rows) no expert is named more than 16 times, a bound that some block reaches.
All inputs are finite; a program needn't handle non-finite values.
Results may differ from a plain program's by a relative error of at most 0.018.
Values may be sent and summed in bfloat16 or wider, within the bound.
A program may use at most 64 MiB of HBM per device.

v0:
```python
import jax
import jax.numpy as jnp
from jax import lax
from jax.sharding import PartitionSpec as P

EPSILON = 1e-06


def norm_rows(values, gain):
    meansq = jnp.mean(values * values, axis=-1, keepdims=True)
    return values * lax.rsqrt(meansq + EPSILON) * gain


def body(
    hidden_in,
    attn_gain,
    query_weight,
    key_weight,
    value_weight,
    query_gain,
    key_gain,
    head_offset,
    key_cache,
    value_cache,
    lengths,
    out_weight,
    expert_gain,
    routes,
    route_weights,
    gate_weight,
    up_weight,
    down_weight,
):
    count_ep = lax.axis_size("ep")
    count_tp = lax.axis_size("tp")
    seqs_here = hidden_in.shape[0]
    width = hidden_in.shape[1]
    head_dim = query_gain.shape[0]
    query_cols = query_weight.shape[1]
    pair_cols = key_weight.shape[1]
    kv_here = pair_cols // head_dim
    groups = query_cols // pair_cols
    cache_len = key_cache.shape[1]
    x_float = hidden_in.astype(jnp.float32)
    normed = norm_rows(x_float, attn_gain).astype(jnp.bfloat16)
    slices = lax.all_to_all(normed, "ep", split_axis=1, concat_axis=0, tiled=True)
    summed = lax.psum_scatter(
        jnp.concatenate(
            [
                jnp.dot(slices, query_weight, preferred_element_type=jnp.float32),
                jnp.dot(slices, key_weight, preferred_element_type=jnp.float32),
                jnp.dot(slices, value_weight, preferred_element_type=jnp.float32),
            ],
            axis=1,
        ),
        "ep",
        scatter_dimension=0,
        tiled=True,
    )
    query_raw = summed[:, :query_cols].astype(jnp.bfloat16)
    key_raw = summed[:, query_cols : query_cols + pair_cols].astype(jnp.bfloat16)
    fresh_values = summed[:, query_cols + pair_cols :].astype(jnp.bfloat16)
    query = norm_rows(
        query_raw.astype(jnp.float32).reshape(seqs_here, query_cols // head_dim, head_dim),
        query_gain,
    ).astype(jnp.bfloat16)
    fresh_keys = norm_rows(
        key_raw.astype(jnp.float32).reshape(seqs_here, kv_here, head_dim), key_gain
    ).astype(jnp.bfloat16)
    grouped = query.reshape(seqs_here, kv_here, groups, head_dim)
    cached_keys = key_cache.reshape(seqs_here, cache_len, kv_here, head_dim)
    cached_values = value_cache.reshape(seqs_here, cache_len, kv_here, head_dim)
    scores = jnp.einsum("bkgd,bskd->bkgs", grouped, cached_keys, preferred_element_type=jnp.float32)
    scores = scores * head_dim ** (-0.5) + head_offset.reshape(kv_here, groups)[None, :, :, None]
    positions = lax.broadcasted_iota(jnp.int32, (1, 1, 1, cache_len), 3)
    live = positions < lengths[:, None, None, None]
    breaks = jnp.where(live, jax.nn.softplus(scores), 0.0)
    suffix = lax.cumsum(breaks, axis=3, reverse=True) - breaks
    stick = jnp.where(live, jnp.exp(jax.nn.log_sigmoid(scores) - suffix), 0.0).astype(jnp.bfloat16)
    attended = jnp.einsum(
        "bkgs,bskd->bkgd", stick, cached_values, preferred_element_type=jnp.float32
    )
    attended = attended.astype(jnp.bfloat16).reshape(seqs_here, query_cols)
    terms = jnp.dot(
        lax.all_gather(attended, "ep", axis=0, tiled=True),
        out_weight,
        preferred_element_type=jnp.float32,
    )
    partial_value = lax.all_to_all(
        terms.astype(jnp.bfloat16), "ep", split_axis=0, concat_axis=1, tiled=True
    ).astype(terms.dtype)
    top = routes.shape[1]
    capacity = seqs_here * top * 2 // count_ep
    slots_all = count_ep * capacity
    flat = routes.reshape(-1)
    onehot = (flat[:, None] == lax.broadcasted_iota(jnp.int32, (1, count_ep), 1)).astype(jnp.int32)
    before = jnp.cumsum(onehot, axis=0) - onehot
    rank = jnp.sum(before * onehot, axis=1)
    slot = flat * capacity + rank
    match = (slot[:, None] == lax.broadcasted_iota(jnp.int32, (1, slots_all), 1)).astype(
        jnp.float32
    )
    match = match.reshape(seqs_here, top, slots_all)
    dispatch = jnp.sum(match, axis=1).astype(jnp.bfloat16)
    combine = jnp.sum(match * route_weights[:, :, None], axis=1)
    share_width = width // count_tp
    col_start = lax.axis_index("tp") * share_width
    projected = lax.psum(partial_value.astype(jnp.bfloat16), "tp").astype(jnp.float32)
    residual = (x_float + projected).astype(jnp.bfloat16)
    expert_in = norm_rows(residual.astype(jnp.float32), expert_gain).astype(jnp.bfloat16)
    outgoing = jnp.einsum(
        "sj,sd->jd", dispatch, expert_in, preferred_element_type=jnp.float32
    ).astype(jnp.bfloat16)
    arrived = lax.all_to_all(outgoing, "ep", split_axis=0, concat_axis=0, tiled=True)
    residual_share = lax.dynamic_slice_in_dim(residual, col_start, share_width, 1)
    gate = jnp.dot(arrived, gate_weight[0], preferred_element_type=jnp.float32)
    upward = jnp.dot(arrived, up_weight[0], preferred_element_type=jnp.float32)
    hidden = (jax.nn.silu(gate) * upward).astype(jnp.bfloat16)
    expert_terms = jnp.dot(hidden, down_weight[0], preferred_element_type=jnp.float32)
    expert_out = lax.psum_scatter(
        expert_terms.astype(jnp.bfloat16), "tp", scatter_dimension=1, tiled=True
    )
    returned = lax.all_to_all(expert_out, "ep", split_axis=0, concat_axis=0, tiled=True)
    mixed = jnp.dot(combine, returned.astype(jnp.float32), precision=lax.Precision.HIGHEST)
    layer_out = (residual_share.astype(jnp.float32) + mixed).astype(jnp.bfloat16)
    return (layer_out, fresh_keys.reshape(seqs_here, pair_cols), fresh_values)


def solution(mesh):
    placed = (
        P("ep", None),
        P(),
        P("ep", "tp"),
        P("ep", "tp"),
        P("ep", "tp"),
        P(),
        P(),
        P("tp"),
        P("ep", None, "tp"),
        P("ep", None, "tp"),
        P("ep"),
        P("tp", "ep"),
        P(),
        P("ep", None),
        P("ep", None),
        P("ep", None, "tp"),
        P("ep", None, "tp"),
        P("ep", "tp", None),
    )
    return jax.shard_map(
        body,
        mesh=mesh,
        in_specs=placed,
        out_specs=(P("ep", "tp"), P("ep", "tp"), P("ep", "tp")),
        check_vma=False,
    )
```

profile of v0, /device:TPU:0, one launch (start us, length us, event | category | flops | bytes accessed | tf_op | source)
XLA Modules:
  0.0 271.5 jit_solution(1524288615958598922)
XLA Ops:
  7.2 0.0 copy-start
  7.2 0.0 copy-start.7
  7.2 0.0 copy-start.9
  7.2 0.0 copy-start.10
  7.2 1.2 fusion.18
  8.4 1.0 fusion.20
  9.4 0.6 copy.57
  10.1 5.2 %all-to-all-start = ((bf16[16,4,1024]{2,0,1:T(8,128)(2,1)}), bf16[16,4,1024]{2,0,1:T(8,128)(2,1)S(1)}, u32[]{:S(2)}, u32[]{:S(2)}) async-start(bf16[16,4,1024]{2,0,1:T(8,128)(2,1)} %bitcast.55), calls=%async_computation | async-start | bytes 262144 | tf_op jit(solution)/shard_map/all_to_all | solution.py:46
  15.3 0.0 reduce-scatter.3.cloned.1.call-start
  15.3 0.8 copy.50
  16.0 0.1 eq.29
  16.1 4.2 %all-to-all-done = bf16[16,4,1024]{2,0,1:T(8,128)(2,1)S(1)} async-done(((bf16[16,4,1024]{2,0,1:T(8,128)(2,1)}), bf16[16,4,1024]{2,0,1:T(8,128)(2,1)S(1)}, u32[]{:S(2)}, u32[]{:S(2)}) %all-to-all-start) | async-done | bytes 131104 | tf_op jit(solution)/shard_map/all_to_all | solution.py:46
  20.3 1.1 fusion.53
  21.4 1.1 fusion.52
  22.6 1.5 fusion.51
  24.1 0.7 pad_maximum_fusion
  24.8 0.0 reduce-scatter.3.cloned.1.call-update
  24.8 0.1 fusion.40
  24.9 0.1 reduce_window_sum.25
  24.9 0.2 select_reduce_fusion.1
  25.1 0.1 reduce_sum.68
  25.2 0.1 copy.51
  25.3 0.1 iota_compare_fusion
  25.4 23.5 %reduce-scatter.3.cloned.1.call-done = f32[16,768]{1,0:T(8,128)} async-done(((f32[64,768]{1,0:T(8,128)}), f32[16,768]{1,0:T(8,128)}) %reduce-scatter.3.cloned.1.call-update) | async-done | bytes 49168 | tf_op jit(solution)/shard_map/reduce_scatter | solution.py:47
  48.9 0.8 convert.6
  49.7 0.1 multiply_reduce_fusion
  49.9 3.5 %fusion.27 = (f32[16,4,1024]{2,1,0:T(4,128)S(1)}, f32[16,4,1024]{2,1,0:T(4,128)S(1)}) fusion(pred[16,1024]{1,0:T(8,128)(4,1)S(1)} %iota_compare_fusion, f32[4]{0:T(128)S(1)} %copy-done.9, bf16[16,1024,128]{2,1,0:T(8,128)(2,1)} %param.26, f32[16,4,128]{2,1,0:T(4,128)S(1)} %reshape.192, f32[128]{0:T(128)S(1)} %copy-done.10, f32[16,4]{1,0:T(8,128)S(1)} %add_rsqrt_fusion), kind=kOutput, calls=%fused_computation.34 | convolution fusion | flops 17391616 | bytes 4768528 | tf_op jit(solution)/shard_map/bkgd,bskd->bkgs/dot_general | solution.py:73
  53.3 0.1 reshape.185
  53.4 79.2 %reduce-window.6 = f32[16,1,4,8,128]{4,3,2,1,0:T(8,128)S(1)} reduce-window(f32[16,1,4,8,128]{4,3,2,1,0:T(8,128)S(1)} %bitcast.65, f32[]{:T(128)} %constant.14.clone.1), window={size=1x1x1x1x128 pad=0_0x0_0x0_0x0_0x0_127}, to_apply=%region_3.0 | reduce-window | flops 8323072 | bytes 524292 | tf_op jit(solution)/shard_map/reduce-window
  132.6 0.1 reshape.186
  132.7 0.3 copy.47
  133.1 0.1 copy.48
  133.2 0.1 broadcast.117
  133.3 0.1 reshape.189
  133.4 0.0 copy-start.3
  133.4 0.0 copy-start.5
  133.4 0.0 copy-start.6
  133.4 3.3 %convolution_convert_fusion.3 = bf16[16,4,128]{2,1,0:T(4,128)(2,1)S(1)} fusion(bf16[16,1024,128]{2,1,0:T(8,128)(2,1)} %param.27, f32[16,4,1024]{2,1,0:T(4,128)S(1)} %reshape.186, f32[16,4,1024]{2,1,0:T(4,128)S(1)} %reshape.189, f32[16,4,1024]{2,1,0:T(4,128)S(1)} %get-tuple-element.8, pred[16,1024]{1,0:T(8,128)(4,1)S(1)} %iota_compare_fusion), kind=kOutput, calls=%fused_computation.14 | convolution fusion | flops 18096128 | bytes 5013504 | tf_op jit(solution)/shard_map/bkgs,bskd->bkgd/dot_general | solution.py:80
  136.8 0.0 copy-start.4
  136.8 8.3 %all_gather.3 = bf16[64,512]{1,0:T(8,128)(2,1)S(1)} all-gather(bf16[16,512]{1,0:T(8,128)(2,1)S(1)} %bitcast.71), channel_id=1, replica_groups=mesh['ep'=4,'tp'=8] {'ep'}, dimensions={0}, use_global_device_ids=true | all-gather | bytes 81920 | tf_op jit(solution)/shard_map/all_gather | solution.py:85
  145.1 0.9 convolution_convert_fusion.2
  146.1 3.3 %all-to-all-start.1 = ((bf16[4,16,1024]{2,1,0:T(8,128)(2,1)}), bf16[4,16,1024]{2,1,0:T(8,128)(2,1)S(1)}, u32[]{:S(2)}, u32[]{:S(2)}) async-start(bf16[4,16,1024]{2,1,0:T(8,128)(2,1)} %bitcast.6), calls=%async_computation.2 | async-start | bytes 262144 | tf_op jit(solution)/shard_map/all_to_all | solution.py:89
  149.4 0.0 all-reduce.2.cloned.1.call-start
  149.5 4.9 %all-to-all-done.1 = bf16[4,16,1024]{2,1,0:T(8,128)(2,1)S(1)} async-done(((bf16[4,16,1024]{2,1,0:T(8,128)(2,1)}), bf16[4,16,1024]{2,1,0:T(8,128)(2,1)S(1)}, u32[]{:S(2)}, u32[]{:S(2)}) %all-to-all-start.1) | async-done | bytes 131104 | tf_op jit(solution)/shard_map/all_to_all | solution.py:89
  154.4 0.7 copy.53
  155.1 0.0 all-reduce.2.cloned.1.call-update
  155.1 0.0 reduce-scatter.5.cloned.1.call-start
  155.1 0.0 copy-done.6
  155.1 0.1 convert_reduce_fusion
  155.2 54.3 %all-reduce.2.cloned.1.call-done = bf16[16,4096]{1,0:T(8,128)(2,1)} async-done(((bf16[16,4096]{1,0:T(8,128)(2,1)}), bf16[16,4096]{1,0:T(8,128)(2,1)}) %all-reduce.2.cloned.1.call-update) | async-done | bytes 131088 | tf_op jit(solution)/shard_map/psum | solution.py:108
  209.6 1.2 fusion.15
  210.8 0.3 convolution_convert_fusion.1
  211.2 10.6 %all_to_all.62 = bf16[4,16,4096]{2,1,0:T(8,128)(2,1)S(1)} all-to-all(bf16[4,16,4096]{2,1,0:T(8,128)(2,1)S(1)} %bitcast.64), channel_id=1, replica_groups=mesh['ep'=4,'tp'=8] {'ep'}, dimensions={0} | all-to-all | bytes 1048576 | tf_op jit(solution)/shard_map/all_to_all | solution.py:114
  221.7 0.5 fusion.3
  222.2 0.0 copy-start.8
  222.2 3.8 %convolution_convert_fusion = bf16[64,4096]{1,0:T(8,128)(2,1)} fusion(bf16[1,256,4096]{2,1,0:T(8,128)(2,1)S(1)} %copy-done, bf16[64,4096]{1,0:T(8,128)(2,1)S(1)} %bitcast.59, bf16[1,4096,256]{2,1,0:T(8,128)(2,1)} %param.34, f32[64,256]{1,0:T(8,128)S(1)} %fusion.3), kind=kOutput, calls=%fused_computation | convolution fusion | flops 268795904 | bytes 5308416 | tf_op jit(solution)/shard_map/dot_general | solution.py:119
  226.0 0.0 reduce-scatter.5.cloned.1.call-update
  226.0 0.1 fusion.43
  226.2 29.6 %reduce-scatter.5.cloned.1.call-done = bf16[64,512]{1,0:T(8,128)(2,1)} async-done(((bf16[64,4096]{1,0:T(8,128)(2,1)}), bf16[64,512]{1,0:T(8,128)(2,1)}) %reduce-scatter.5.cloned.1.call-update) | async-done | bytes 65552 | tf_op jit(solution)/shard_map/reduce_scatter | solution.py:120
  255.8 3.5 %all-to-all-start.3 = ((bf16[4,16,512]{2,1,0:T(8,128)(2,1)}), bf16[4,16,512]{2,1,0:T(8,128)(2,1)S(1)}, u32[]{:S(2)}, u32[]{:S(2)}) async-start(bf16[4,16,512]{2,1,0:T(8,128)(2,1)} %bitcast.72), calls=%async_computation.5 | async-start | bytes 131072 | tf_op jit(solution)/shard_map/all_to_all | solution.py:123
  259.3 0.7 fusion.45
  260.0 0.6 slice.27
  260.6 3.6 %all-to-all-done.3 = bf16[4,16,512]{2,1,0:T(8,128)(2,1)S(1)} async-done(((bf16[4,16,512]{2,1,0:T(8,128)(2,1)}), bf16[4,16,512]{2,1,0:T(8,128)(2,1)S(1)}, u32[]{:S(2)}, u32[]{:S(2)}) %all-to-all-start.3) | async-done | bytes 65568 | tf_op jit(solution)/shard_map/all_to_all | solution.py:123
  264.2 0.8 fusion.14
  (22 shorter events, 0.1 us)
Async XLA Ops:
  7.2 215.0 %copy-start = (bf16[1,256,4096]{2,1,0:T(8,128)(2,1)S(1)}, bf16[1,256,4096]{2,1,0:T(8,128)(2,1)}, u32[]{:S(2)}) copy-start(bf16[1,256,4096]{2,1,0:T(8,128)(2,1)} %param.35) | copy-start | bytes 6291460
  7.2 18.1 %copy-start.7 = (s32[16]{0:T(128)S(1)}, s32[16]{0:T(128)}, u32[]{:S(2)}) copy-start(s32[16]{0:T(128)} %param.28) | copy-start | bytes 196
  7.2 42.6 %copy-start.9 = (f32[4]{0:T(128)S(1)}, f32[4]{0:T(128)}, u32[]{:S(2)}) copy-start(f32[4]{0:T(128)} %param.25) | copy-start | bytes 52
  7.2 42.6 %copy-start.10 = (f32[128]{0:T(128)S(1)}, f32[128]{0:T(128)}, u32[]{:S(2)}) copy-start(f32[128]{0:T(128)} %param.23) | copy-start | bytes 1540
  10.1 10.2 %all-to-all-start = ((bf16[16,4,1024]{2,0,1:T(8,128)(2,1)}), bf16[16,4,1024]{2,0,1:T(8,128)(2,1)S(1)}, u32[]{:S(2)}, u32[]{:S(2)}) async-start(bf16[16,4,1024]{2,0,1:T(8,128)(2,1)} %bitcast.55), calls=%async_computation | async-start | bytes 262144 | tf_op jit(solution)/shard_map/all_to_all | solution.py:46
  15.3 33.6 %reduce-scatter.3.cloned.1.call-start = ((), (), s32[]{:S(2)}) async-start(), calls=%async_computation.6 | async-start | bytes 245760 | tf_op jit(solution)/shard_map/reduce_scatter | solution.py:47
  133.4 11.7 %copy-start.3 = (bf16[512,1024]{1,0:T(8,128)(2,1)S(1)}, bf16[512,1024]{1,0:T(8,128)(2,1)}, u32[]{:S(2)}) copy-start(bf16[512,1024]{1,0:T(8,128)(2,1)} %param.29) | copy-start | bytes 3145732
  133.4 16.1 %copy-start.5 = (s32[16,2]{0,1:T(2,128)S(1)}, s32[16,2]{0,1:T(2,128)}, u32[]{:S(2)}) copy-start(s32[16,2]{0,1:T(2,128)} %param.31) | copy-start | bytes 388
  133.4 21.7 %copy-start.6 = (f32[16,2]{0,1:T(2,128)S(1)}, f32[16,2]{0,1:T(2,128)}, u32[]{:S(2)}) copy-start(f32[16,2]{0,1:T(2,128)} %param.32) | copy-start | bytes 388
  136.8 72.8 %copy-start.2 = (bf16[16,4096]{1,0:T(8,128)(2,1)S(1)}, bf16[16,4096]{1,0:T(8,128)(2,1)}, u32[]{:S(2)}) copy-start(bf16[16,4096]{1,0:T(8,128)(2,1)} %param.18) | copy-start | bytes 393220
  136.8 74.0 %copy-start.4 = (f32[4096]{0:T(1024)S(1)}, f32[4096]{0:T(1024)}, u32[]{:S(2)}) copy-start(f32[4096]{0:T(1024)} %param.30) | copy-start | bytes 49156
  146.1 8.3 %all-to-all-start.1 = ((bf16[4,16,1024]{2,1,0:T(8,128)(2,1)}), bf16[4,16,1024]{2,1,0:T(8,128)(2,1)S(1)}, u32[]{:S(2)}, u32[]{:S(2)}) async-start(bf16[4,16,1024]{2,1,0:T(8,128)(2,1)} %bitcast.6), calls=%async_computation.2 | async-start | bytes 262144 | tf_op jit(solution)/shard_map/all_to_all | solution.py:89
  149.4 60.2 %all-reduce.2.cloned.1.call-start = ((), (), s32[]{:S(2)}) async-start(), calls=%async_computation.7 | async-start | bytes 262144 | tf_op jit(solution)/shard_map/psum | solution.py:108
  155.1 100.7 %reduce-scatter.5.cloned.1.call-start = ((), (), s32[]{:S(2)}) async-start(), calls=%async_computation.8 | async-start | bytes 589824 | tf_op jit(solution)/shard_map/reduce_scatter | solution.py:120
  209.6 12.2 %copy-start.1 = (bf16[1,4096,256]{2,1,0:T(8,128)(2,1)S(1)}, bf16[1,4096,256]{2,1,0:T(8,128)(2,1)}, u32[]{:S(2)}) copy-start(bf16[1,4096,256]{2,1,0:T(8,128)(2,1)} %param.33) | copy-start | bytes 6291460
  222.2 37.1 %copy-start.8 = (f32[128]{0:T(128)S(1)}, f32[128]{0:T(128)}, u32[]{:S(2)}) copy-start(f32[128]{0:T(128)} %param.24) | copy-start | bytes 1540
  255.8 8.4 %all-to-all-start.3 = ((bf16[4,16,512]{2,1,0:T(8,128)(2,1)}), bf16[4,16,512]{2,1,0:T(8,128)(2,1)S(1)}, u32[]{:S(2)}, u32[]{:S(2)}) async-start(bf16[4,16,512]{2,1,0:T(8,128)(2,1)} %bitcast.72), calls=%async_computation.5 | async-start | bytes 131072 | tf_op jit(solution)/shard_map/all_to_all | solution.py:123
Sparse Core Ops, SparseCore 0:
  24.9 23.9 reduce-scatter.2
  155.2 54.3 all-reduce.1
  226.2 29.5 reduce-scatter.4
where the time goes:
time: 272 us; the launch traced here: 271 us
  waiting for transfers between devices  120 us (44%)
  other arithmetic  85.6 us (31%)
  blocking collectives  18.9 us (7%)
  matrix products  16.9 us (6%)
  between operations  14 us (5%)
  starting transfers between devices  12.1 us (4%)
  local copies, waits for them, and re-layouts  3.78 us (1%)
    another operation x3, other arithmetic  80.1 us
    psum x1, waiting for transfers between devices, body(): lax.psum(partial_value.astype(jnp.bfloat16), 'tp').astype(jnp.float32)  54.3 us
    reduce_scatter x1, waiting for transfers between devices, body(): lax.psum_scatter(expert_terms.astype(jnp.bfloat16), 'tp', scatter_dimensi...  29.6 us
    reduce_scatter x1, waiting for transfers between devices, body(): lax.psum_scatter(jnp.concatenate([jnp.dot(slices, query_weight, preferred...  23.5 us
    all_to_all x1, blocking collectives, body(): lax.all_to_all(outgoing, 'ep', split_axis=0, concat_axis=0, tiled=True)  10.6 us
    all_gather x1, blocking collectives, body(): lax.all_gather(attended, 'ep', axis=0, tiled=True)  8.33 us
  transfers between devices with their start and end apart: 6, of which 6 were waited for; matrix products, arithmetic and copies ran while one was open for 1% of the time, Pallas kernels for 0%

commit v1 on v0

v1 whole, which is shorter than its diff:
```python
import functools

import jax
import jax.numpy as jnp
from jax import lax
from jax.experimental import pallas as pl
from jax.experimental.pallas import tpu as pltpu
from jax.sharding import PartitionSpec as P

EPSILON = 1e-06
MESH = pl.DeviceIdType.MESH
F32 = jnp.float32
BF16 = jnp.bfloat16


def dot(a, b):
    return jnp.dot(a, b, preferred_element_type=F32)


def kernel(
    n_ep,
    n_tp,
    hid,
    attn_gain,
    wq_h,
    wk_h,
    wv_h,
    query_gain,
    key_gain,
    offset_s,
    kc_h,
    vc_h,
    lengths_s,
    wo_h,
    expert_gain,
    routes,
    route_weights,
    wg_h,
    wu_h,
    wd_h,
    out,
    fresh_k,
    fresh_v,
    hid_v,
    wq,
    wk,
    wv,
    kc,
    vc,
    wo,
    wg,
    wu,
    wd,
    xs,
    xf,
    part_s,
    part_r,
    q_s,
    z_s,
    st_s,
    o_s,
    att,
    p_s,
    p_r,
    res,
    y_s,
    y_r,
    m_s,
    m_r,
    local_sem,
    xs_sem,
    part_sem,
    att_sem,
    p_sem,
    res_sem,
    ep_sem,
    y_sem,
    m_sem,
):
    e = lax.axis_index("ep")
    t = lax.axis_index("tp")
    seqs, width = hid.shape
    feats = xs.shape[2]
    hd = query_gain.shape[1]
    qc = wq.shape[1]
    pc = wk.shape[1]
    heads = qc // hd
    kv = pc // hd
    groups = heads // kv
    cache = kc.shape[1]
    tokens = seqs * n_ep
    rows = tokens // n_tp
    per = seqs // rows
    share = width // n_tp

    def up_ep(j):
        return lax.rem(e + j, n_ep)

    def down_ep(j):
        return lax.rem(e + n_ep - j, n_ep)

    def up_tp(j):
        return lax.rem(t + j, n_tp)

    def down_tp(j):
        return lax.rem(t + n_tp - j, n_tp)

    def send(src, dst, sems, j, device):
        copy = pltpu.make_async_remote_copy(
            src_ref=src,
            dst_ref=dst,
            send_sem=sems.at[0, j],
            recv_sem=sems.at[1, j],
            device_id=device,
            device_id_type=MESH,
        )
        copy.start()
        return copy

    pairs = [
        (hid, hid_v),
        (hid.at[:, pl.ds(pl.multiple_of(e * feats, feats), feats)], xs.at[0]),
        (wq_h, wq),
        (wk_h, wk),
        (wv_h, wv),
        (kc_h, kc),
        (vc_h, vc),
        (wo_h, wo),
        (wg_h, wg),
        (wu_h, wu),
        (wd_h, wd),
    ]
    copies = [pltpu.make_async_copy(a, b, local_sem.at[i]) for i, (a, b) in enumerate(pairs)]
    for copy in copies:
        copy.start()
    c_hid, c_x0, c_q, c_k, c_v, c_kc, c_vc, c_wo, c_wg, c_wu, c_wd = copies

    barrier = pltpu.get_barrier_semaphore()
    for j in range(1, n_ep):
        pl.semaphore_signal(barrier, inc=1, device_id=(up_ep(j), t), device_id_type=MESH)
    for j in range(1, n_tp):
        pl.semaphore_signal(barrier, inc=1, device_id=(e, up_tp(j)), device_id_type=MESH)
    pl.semaphore_wait(barrier, n_ep + n_tp - 2)

    sent = []
    for j in range(1, n_ep):
        peer = up_ep(j)
        cols = pl.ds(pl.multiple_of(peer * feats, feats), feats)
        sent.append(send(hid.at[:, cols], xs.at[j], xs_sem, j - 1, (peer, t)))
    c_hid.wait()
    x = hid_v[...].astype(F32)
    scale = lax.rsqrt(jnp.mean(x * x, axis=1, keepdims=True) + EPSILON)
    c_x0.wait()
    gain = attn_gain[:, pl.ds(pl.multiple_of(e * feats, feats), feats)]
    for j in range(n_ep):
        if j > 0:
            sent[j - 1].wait()
        xj = xs[j].astype(F32)
        xf[j] = xj.reshape(per, rows, feats)
    lhs = jnp.concatenate([(xs[j].astype(F32) * gain).astype(BF16) for j in range(n_ep)], axis=0)
    c_q.wait()
    c_k.wait()
    c_v.wait()
    sums = jnp.concatenate([dot(lhs, wq[...]), dot(lhs, wk[...]), dot(lhs, wv[...])], axis=1)
    for j in range(n_ep):
        part_s[j] = sums[j * seqs : (j + 1) * seqs]
    sent = [send(part_s.at[j], part_r.at[j], part_sem, j - 1, (down_ep(j), t)) for j in range(1, n_ep)]
    total = part_s[0]
    for j in range(1, n_ep):
        sent[j - 1].wait()
        total = total + part_r[j]
    total = total * scale
    raw = total.astype(BF16)
    fresh_v[...] = raw[:, qc + pc :]
    rawf = raw.astype(F32)

    def head_norm(vals, g):
        return vals * lax.rsqrt(jnp.mean(vals * vals, axis=1, keepdims=True) + EPSILON) * g

    for k in range(kv):
        cols = slice(qc + k * hd, qc + (k + 1) * hd)
        fresh_k[:, k * hd : (k + 1) * hd] = head_norm(rawf[:, cols], key_gain[...]).astype(BF16)
    q_s[...] = jnp.zeros_like(q_s)
    for h in range(heads):
        q_s[h // groups, :, h % groups, :] = head_norm(rawf[:, h * hd : (h + 1) * hd], query_gain[...])

    lines = q_s.shape[2]
    span = min(256, cache)
    later = (
        lax.broadcasted_iota(jnp.int32, (span, span), 0)
        > lax.broadcasted_iota(jnp.int32, (span, span), 1)
    ).astype(BF16)
    place = lax.broadcasted_iota(jnp.int32, (1, lines, cache), 2)
    line = lax.broadcasted_iota(jnp.int32, (1, lines, 1), 1)
    inv = hd ** (-0.5)
    c_kc.wait()
    for k in range(kv):
        shift = jnp.zeros((1, lines, 1), F32)
        for g in range(groups):
            shift = jnp.where(line == g, offset_s[k * groups + g], shift)

        def score(b, carry, k=k, shift=shift):
            qb = q_s[k, b].astype(BF16)
            z = lax.dot_general(
                qb,
                kc[b, :, k * hd : (k + 1) * hd],
                (((1,), (1,)), ((), ())),
                preferred_element_type=F32,
            )
            z_s[pl.ds(b, 1)] = (z * inv)[None] + shift
            return carry

        lax.fori_loop(0, seqs, score, 0, unroll=True)

        limit = jnp.concatenate(
            [jnp.full((1, lines, 1), lengths_s[b], jnp.int32) for b in range(seqs)], axis=0
        )
        carry = jnp.zeros((seqs * lines, 1), F32)
        for c in reversed(range(cache // span)):
            z = z_s[:, :, c * span : (c + 1) * span]
            live = place[:, :, c * span : (c + 1) * span] < limit
            soft = jnp.log1p(jnp.exp(-jnp.abs(z)))
            breaks = jnp.where(live, jnp.maximum(z, 0.0) + soft, 0.0).reshape(seqs * lines, span)
            logsig = jnp.minimum(z, 0.0) - soft
            high = breaks.astype(BF16)
            mid = (breaks - high.astype(F32)).astype(BF16)
            suffix = dot(high, later) + dot(mid, later)
            after = (suffix + carry).reshape(seqs, lines, span)
            stick = jnp.where(live, jnp.exp(logsig - after), 0.0)
            st_s[:, :, c * span : (c + 1) * span] = stick
            carry = carry + suffix[:, 0:1] + breaks[:, 0:1]
        if k == 0:
            c_vc.wait()

        def mix(b, carry, k=k):
            o_s[k, pl.ds(b, 1)] = dot(st_s[b].astype(BF16), vc[b, :, k * hd : (k + 1) * hd])[None]
            return carry

        lax.fori_loop(0, seqs, mix, 0, unroll=True)
    for h in range(heads):
        att[0, :, h * hd : (h + 1) * hd] = o_s[h // groups, :, h % groups, :].astype(BF16)

    sent = [send(att.at[0], att.at[j], att_sem, j - 1, (up_ep(j), t)) for j in range(1, n_ep)]
    c_wo.wait()
    for j in range(n_ep):
        if j > 0:
            sent[j - 1].wait()
        block = dot(att[j], wo[...]).reshape(per, rows, feats).astype(BF16)
        p_s[pl.ds(down_ep(j) * per, per)] = block
    sent = [send(p_s.at[up_tp(j)], p_r.at[j], p_sem, j - 1, (e, up_tp(j))) for j in range(1, n_tp)]
    total = p_s[t].astype(F32)
    for j in range(1, n_tp):
        sent[j - 1].wait()
        total = total + p_r[j].astype(F32)
    owner = t // per
    slot = lax.rem(e + n_ep - owner, n_ep)
    res[0, t] = (xf[slot, lax.rem(t, per)] + total).astype(BF16)
    sent = [send(res.at[0, t], res.at[0, t], res_sem, j - 1, (e, up_tp(j))) for j in range(1, n_tp)]
    for copy in sent:
        copy.wait()
    sent = [send(res.at[0], res.at[j], ep_sem, j - 1, (up_ep(j), t)) for j in range(1, n_ep)]

    c_wg.wait()
    c_wu.wait()
    square = jnp.zeros((tokens, 1), F32)
    gate = jnp.zeros((tokens, wg.shape[2]), F32)
    upward = jnp.zeros((tokens, wg.shape[2]), F32)
    for j in range(n_ep):
        if j > 0:
            sent[j - 1].wait()
        at = pl.ds(pl.multiple_of(down_ep(j) * feats, feats), feats)
        r = res[j].astype(F32).reshape(tokens, feats)
        square = square + jnp.sum(r * r, axis=1, keepdims=True)
        r = (r * expert_gain[:, at]).astype(BF16)
        gate = gate + dot(r, wg[0, at, :])
        upward = upward + dot(r, wu[0, at, :])
    scale = lax.rsqrt(square / width + EPSILON)
    gate = gate * scale
    hidden = (gate * jax.nn.sigmoid(gate) * (upward * scale)).astype(BF16)
    c_wd.wait()
    for c in range(n_tp):
        block = dot(hidden, wd[0, :, c * share : (c + 1) * share]).astype(BF16)
        y_s[:, :, c * share : (c + 1) * share] = block.reshape(n_ep, seqs, share)

    sent = [send(y_s.at[up_ep(j)], y_r.at[j], y_sem, j - 1, (up_ep(j), t)) for j in range(1, n_ep)]
    mixed = jnp.zeros((seqs, width), F32)
    for j in range(n_ep):
        expert = down_ep(j)
        weight = jnp.sum(
            jnp.where(routes[...] == expert, route_weights[...], 0.0), axis=1, keepdims=True
        )
        if j > 0:
            sent[j - 1].wait()
            terms = y_r[j]
        else:
            terms = y_s[e]
        mixed = mixed + weight * terms.astype(F32)
    for c in range(n_tp):
        m_s[c] = mixed[:, c * share : (c + 1) * share].astype(BF16)
    sent = [send(m_s.at[up_tp(j)], m_r.at[j], m_sem, j - 1, (e, up_tp(j))) for j in range(1, n_tp)]
    holder = t * share // feats
    slot = lax.rem(e + n_ep - holder, n_ep)
    start = pl.multiple_of(lax.rem(t * share, feats), share)
    total = res[slot, pl.ds(e * per, per), :, pl.ds(start, share)].astype(F32).reshape(seqs, share)
    total = total + m_s[t].astype(F32)
    for j in range(1, n_tp):
        sent[j - 1].wait()
        total = total + m_r[j].astype(F32)
    out[...] = total.astype(BF16)


def body(
    hidden_in,
    attn_gain,
    query_weight,
    key_weight,
    value_weight,
    query_gain,
    key_gain,
    head_offset,
    key_cache,
    value_cache,
    lengths,
    out_weight,
    expert_gain,
    routes,
    route_weights,
    gate_weight,
    up_weight,
    down_weight,
):
    n_ep = lax.axis_size("ep")
    n_tp = lax.axis_size("tp")
    seqs, width = hidden_in.shape
    hd = query_gain.shape[0]
    feats, qc = query_weight.shape
    pc = key_weight.shape[1]
    kv = pc // hd
    lines = -(-(qc // pc) // 8) * 8
    cache = key_cache.shape[1]
    cols = out_weight.shape[1]
    tokens = seqs * n_ep
    rows = tokens // n_tp
    share = width // n_tp
    any_, vmem, smem = (
        pl.BlockSpec(memory_space=pl.ANY),
        pl.BlockSpec(memory_space=pltpu.VMEM),
        pl.BlockSpec(memory_space=pltpu.SMEM),
    )
    dma = pltpu.SemaphoreType.DMA

    def like(a):
        return pltpu.VMEM(a.shape, a.dtype)

    return pl.pallas_call(
        functools.partial(kernel, n_ep, n_tp),
        out_shape=(
            jax.ShapeDtypeStruct((seqs, share), BF16),
            jax.ShapeDtypeStruct((seqs, pc), BF16),
            jax.ShapeDtypeStruct((seqs, pc), BF16),
        ),
        in_specs=[
            any_, vmem, any_, any_, any_, vmem, vmem, smem, any_, any_, smem, any_, vmem, vmem,
            vmem, any_, any_, any_,
        ],
        out_specs=(vmem, vmem, vmem),
        scratch_shapes=[
            like(hidden_in),
            like(query_weight),
            like(key_weight),
            like(value_weight),
            like(key_cache),
            like(value_cache),
            like(out_weight),
            like(gate_weight),
            like(up_weight),
            like(down_weight),
            pltpu.VMEM((n_ep, seqs, feats), BF16),
            pltpu.VMEM((n_ep, seqs // rows, rows, feats), F32),
            pltpu.VMEM((n_ep, seqs, qc + 2 * pc), F32),
            pltpu.VMEM((n_ep, seqs, qc + 2 * pc), F32),
            pltpu.VMEM((kv, seqs, lines, hd), F32),
            pltpu.VMEM((seqs, lines, cache), F32),
            pltpu.VMEM((seqs, lines, cache), F32),
            pltpu.VMEM((kv, seqs, lines, hd), F32),
            pltpu.VMEM((n_ep, seqs, qc), BF16),
            pltpu.VMEM((n_tp, rows, cols), BF16),
            pltpu.VMEM((n_tp, rows, cols), BF16),
            pltpu.VMEM((n_ep, n_tp, rows, cols), BF16),
            pltpu.VMEM((n_ep, seqs, width), BF16),
            pltpu.VMEM((n_ep, seqs, width), BF16),
            pltpu.VMEM((n_tp, seqs, share), BF16),
            pltpu.VMEM((n_tp, seqs, share), BF16),
            dma((11,)),
            dma((2, n_ep - 1)),
            dma((2, n_ep - 1)),
            dma((2, n_ep - 1)),
            dma((2, n_tp - 1)),
            dma((2, n_tp - 1)),
            dma((2, n_ep - 1)),
            dma((2, n_ep - 1)),
            dma((2, n_tp - 1)),
        ],
        compiler_params=pltpu.CompilerParams(
            collective_id=0, has_side_effects=True, vmem_limit_bytes=60 * 2**20
        ),
    )(
        hidden_in,
        attn_gain.reshape(1, -1),
        query_weight,
        key_weight,
        value_weight,
        query_gain.reshape(1, -1),
        key_gain.reshape(1, -1),
        head_offset,
        key_cache,
        value_cache,
        lengths,
        out_weight,
        expert_gain.reshape(1, -1),
        routes,
        route_weights,
        gate_weight,
        up_weight,
        down_weight,
    )


def solution(mesh):
    placed = (
        P("ep", None),
        P(),
        P("ep", "tp"),
        P("ep", "tp"),
        P("ep", "tp"),
        P(),
        P(),
        P("tp"),
        P("ep", None, "tp"),
        P("ep", None, "tp"),
        P("ep"),
        P("tp", "ep"),
        P(),
        P("ep", None),
        P("ep", None),
        P("ep", None, "tp"),
        P("ep", None, "tp"),
        P("ep", "tp", None),
    )
    return jax.shard_map(
        body,
        mesh=mesh,
        in_specs=placed,
        out_specs=(P("ep", "tp"), P("ep", "tp"), P("ep", "tp")),
        check_vma=False,
    )
```

time: 272 us -> 58 us (0.21)
  waiting for transfers between devices: 120 us -> 0 us
  other arithmetic: 85.6 us -> 0 us
  Pallas kernels: 0 us -> 50.4 us
  blocking collectives: 18.9 us -> 0 us
  matrix products: 16.9 us -> 0 us
  between operations: 14 us -> 0.64 us
  starting transfers between devices: 12.1 us -> 0 us
  local copies, waits for them, and re-layouts: 3.78 us -> 6.56 us
    another operation x4 -> x0, other arithmetic: 80.1 us -> none
    psum x1 -> x0, waiting for transfers between devices: 54.3 us -> none  [body(): lax.psum(partial_value.astype(jnp.bfloat16), 'tp').astype(jnp.float32)]
    reduce_scatter x2 -> x0, waiting for transfers between devices: 53.1 us -> none  [the longest x1 29.6 us: body(): lax.psum_scatter(expert_terms.astype(jnp.bfloat16), 'tp', scatter_dimensi...]
    pallas_call x0 -> x1, Pallas kernels: none -> 50.4 us  [body(): pl.pallas_call(functools.partial(kernel, n_ep, n_tp), out_shape=(jax.Shap...]
    dot_general x10 -> x0, matrix products: 16.9 us -> none  [the longest x1 3.79 us: body(): jnp.dot(hidden, down_weight[0], preferred_element_type=jnp.float32)]
    all_to_all x3 -> x0, waiting for transfers between devices: 12.7 us -> none  [the longest x1 4.92 us: body(): lax.all_to_all(terms.astype(jnp.bfloat16), 'ep', split_axis=0, concat_axi...]
    all_to_all x3 -> x0, starting transfers between devices: 12.1 us -> none  [the longest x1 5.19 us: body(): lax.all_to_all(normed, 'ep', split_axis=1, concat_axis=0, tiled=True)]
    all_to_all x1 -> x0, blocking collectives: 10.6 us -> none  [body(): lax.all_to_all(outgoing, 'ep', split_axis=0, concat_axis=0, tiled=True)]
  transfers between devices with their start and end apart: 6 -> 0, of which waited for: 6 -> 0; matrix products, arithmetic and copies ran while one was open for 1% -> 0% of each run, Pallas kernels for 0% -> 0%
where the time goes in v1:
time: 58 us; the launch traced here: 57.6 us
  Pallas kernels  50.4 us (87%)
  local copies, waits for them, and re-layouts  6.56 us (11%)
  between operations  0.64 us (1%)
    pallas_call x1, Pallas kernels, body(): pl.pallas_call(functools.partial(kernel, n_ep, n_tp), out_shape=(jax.Shap...  50.4 us
    unnamed x5, local copies, waits for them, and re-layouts  6.56 us

profile of v1, /device:TPU:0, one launch (start us, length us, event | category | flops | bytes accessed | tf_op | source)
XLA Modules:
  0.0 57.6 jit_solution(8421643441564868442)
XLA Ops:
  0.6 1.4 %copy.21.routes = s32[16,2]{1,0:T(8,128)} copy(s32[16,2]{0,1:T(2,128)} %param.31) | data formatting | bytes 256 | tf_op args[13]
  2.0 1.3 %copy.22.route_weights = f32[16,2]{1,0:T(8,128)} copy(f32[16,2]{0,1:T(2,128)} %param.32) | data formatting | bytes 256 | tf_op args[14]
  3.3 50.4 %shard_map.193 = (bf16[16,512]{1,0:T(8,128)(2,1)}, bf16[16,128]{1,0:T(8,128)(2,1)}, bf16[16,128]{1,0:T(8,128)(2,1)}) custom-call(bf16[16,4096]{1,0:T(8,128)(2,1)} %hid.1, f32[1,4096]{1,0:T(1,128)} %bitcast.4, bf16[1024,512]{1,0:T(8,128)(2,1)} %wq_h.1, bf16[1024,128]{1,0:T(8,128)(2,1)} %wk_h.1, bf16[1024,128]{1,0:T(8,128)(2,1)} %wv_h.1, f32[1,128]{1,0:T(1,128)} %bitcast.6, ...), custom_call_target="tpu_custom_call" | custom-call | tf_op jit(solution)/shard_map/pallas_call | solution.py:355
  53.7 1.3 %copy.26 = bf16[16,512]{1,0:T(8,128)(2,1)} copy(bf16[16,512]{1,0:T(8,128)(2,1)} %get-tuple-element.6) | data formatting | bytes 32768
  55.1 1.3 %copy.27 = bf16[16,128]{1,0:T(8,128)(2,1)} copy(bf16[16,128]{1,0:T(8,128)(2,1)} %get-tuple-element.7) | data formatting | bytes 8192
  56.3 1.3 %copy.28 = bf16[16,128]{1,0:T(8,128)(2,1)} copy(bf16[16,128]{1,0:T(8,128)(2,1)} %get-tuple-element.8) | data formatting | bytes 8192

commit v2 on v1

--- a/solution.py
+++ b/solution.py
@@ -63,6 +63,8 @@
     p_s,
     p_r,
     res,
+    d_s,
+    d_r,
     y_s,
     y_r,
     m_s,
@@ -74,6 +76,8 @@
     p_sem,
     res_sem,
     ep_sem,
+    pair_sem,
+    d_sem,
     y_sem,
     m_sem,
 ):
@@ -140,14 +144,23 @@
         pl.semaphore_signal(barrier, inc=1, device_id=(up_ep(j), t), device_id_type=MESH)
     for j in range(1, n_tp):
         pl.semaphore_signal(barrier, inc=1, device_id=(e, up_tp(j)), device_id_type=MESH)
+    weights = []
+    same = lax.broadcasted_iota(jnp.int32, (seqs, seqs), 0) == lax.broadcasted_iota(
+        jnp.int32, (seqs, seqs), 1
+    )
+    for j in range(n_ep):
+        flat = jnp.sum(
+            jnp.where(routes[...] == down_ep(j), route_weights[...], 0.0), axis=0, keepdims=True
+        )
+        weights.append(jnp.sum(jnp.where(same, flat, 0.0), axis=1, keepdims=True))
+    c_hid.wait()
     pl.semaphore_wait(barrier, n_ep + n_tp - 2)
 
     sent = []
     for j in range(1, n_ep):
         peer = up_ep(j)
         cols = pl.ds(pl.multiple_of(peer * feats, feats), feats)
-        sent.append(send(hid.at[:, cols], xs.at[j], xs_sem, j - 1, (peer, t)))
-    c_hid.wait()
+        sent.append(send(hid_v.at[:, cols], xs.at[j], xs_sem, j - 1, (peer, t)))
     x = hid_v[...].astype(F32)
     scale = lax.rsqrt(jnp.mean(x * x, axis=1, keepdims=True) + EPSILON)
     c_x0.wait()
@@ -163,12 +176,12 @@
     c_v.wait()
     sums = jnp.concatenate([dot(lhs, wq[...]), dot(lhs, wk[...]), dot(lhs, wv[...])], axis=1)
     for j in range(n_ep):
-        part_s[j] = sums[j * seqs : (j + 1) * seqs]
+        part_s[j] = sums[j * seqs : (j + 1) * seqs].astype(BF16)
     sent = [send(part_s.at[j], part_r.at[j], part_sem, j - 1, (down_ep(j), t)) for j in range(1, n_ep)]
-    total = part_s[0]
+    total = sums[:seqs]
     for j in range(1, n_ep):
         sent[j - 1].wait()
-        total = total + part_r[j]
+        total = total + part_r[j].astype(F32)
     total = total * scale
     raw = total.astype(BF16)
     fresh_v[...] = raw[:, qc + pc :]
@@ -255,19 +268,51 @@
     owner = t // per
     slot = lax.rem(e + n_ep - owner, n_ep)
     res[0, t] = (xf[slot, lax.rem(t, per)] + total).astype(BF16)
-    sent = [send(res.at[0, t], res.at[0, t], res_sem, j - 1, (e, up_tp(j))) for j in range(1, n_tp)]
-    for copy in sent:
-        copy.wait()
-    sent = [send(res.at[0], res.at[j], ep_sem, j - 1, (up_ep(j), t)) for j in range(1, n_ep)]
+
+    n_z = n_tp // 2
+    z = t // 2
+    core = lax.rem(t, 2)
+    other = (e, z * 2 + 1 - core)
+
+    def at_z(d):
+        return lax.rem(z + d, n_z) * 2 + core
+
+    def back_z(d):
+        return lax.rem(z + n_z - d, n_z) * 2 + core
+
+    along = [None] + [
+        send(res.at[0, t], res.at[0, t], res_sem, d - 1, (e, at_z(d))) for d in range(1, n_z)
+    ]
+    across = {}
+    paired = []
+    for d in range(n_z):
+        if d > 0:
+            along[d].wait()
+        piece = back_z(d)
+        for j in range(1, n_ep):
+            across[d, j] = send(
+                res.at[0, piece],
+                res.at[j, piece],
+                ep_sem,
+                d * (n_ep - 1) + j - 1,
+                (up_ep(j), t),
+            )
+        paired.append(send(res.at[0, piece], res.at[0, piece], pair_sem, d, other))
+    for d in range(n_z):
+        piece = back_z(d)
+        for j in range(1, n_ep):
+            across[d, j].wait()
+            at = d * (n_ep - 1) + j - 1 + n_z
+            paired.append(send(res.at[j, piece], res.at[j, piece], pair_sem, at, other))
 
     c_wg.wait()
     c_wu.wait()
     square = jnp.zeros((tokens, 1), F32)
     gate = jnp.zeros((tokens, wg.shape[2]), F32)
     upward = jnp.zeros((tokens, wg.shape[2]), F32)
+    for copy in paired:
+        copy.wait()
     for j in range(n_ep):
-        if j > 0:
-            sent[j - 1].wait()
         at = pl.ds(pl.multiple_of(down_ep(j) * feats, feats), feats)
         r = res[j].astype(F32).reshape(tokens, feats)
         square = square + jnp.sum(r * r, axis=1, keepdims=True)
@@ -278,35 +323,53 @@
     gate = gate * scale
     hidden = (gate * jax.nn.sigmoid(gate) * (upward * scale)).astype(BF16)
     c_wd.wait()
-    for c in range(n_tp):
-        block = dot(hidden, wd[0, :, c * share : (c + 1) * share]).astype(BF16)
-        y_s[:, :, c * share : (c + 1) * share] = block.reshape(n_ep, seqs, share)
-
-    sent = [send(y_s.at[up_ep(j)], y_r.at[j], y_sem, j - 1, (up_ep(j), t)) for j in range(1, n_ep)]
-    mixed = jnp.zeros((seqs, width), F32)
-    for j in range(n_ep):
-        expert = down_ep(j)
-        weight = jnp.sum(
-            jnp.where(routes[...] == expert, route_weights[...], 0.0), axis=1, keepdims=True
-        )
-        if j > 0:
-            sent[j - 1].wait()
-            terms = y_r[j]
-        else:
-            terms = y_s[e]
-        mixed = mixed + weight * terms.astype(F32)
-    for c in range(n_tp):
-        m_s[c] = mixed[:, c * share : (c + 1) * share].astype(BF16)
-    sent = [send(m_s.at[up_tp(j)], m_r.at[j], m_sem, j - 1, (e, up_tp(j))) for j in range(1, n_tp)]
+
+    def down(block):
+        at = pl.ds(pl.multiple_of(block * share, share), share)
+        return dot(hidden, wd[0, :, at])
+
+    turns = list(range(1, n_z)) + [0]
+    paired = {}
+    for d in turns:
+        d_s[d] = down(lax.rem(z + d, n_z) * 2 + 1 - core).astype(BF16).reshape(n_ep, seqs, share)
+        paired[d] = send(d_s.at[d], d_r.at[d], d_sem, d, other)
+    across = {}
+    for d in turns:
+        mine = down(at_z(d)).reshape(n_ep, seqs, share)
+        paired[d].wait()
+        y_s[d] = (mine + d_r[d].astype(F32)).astype(BF16)
+        for j in range(1, n_ep):
+            across[d, j] = send(
+                y_s.at[d, up_ep(j)],
+                y_r.at[d, j],
+                y_sem,
+                d * (n_ep - 1) + j - 1,
+                (up_ep(j), t),
+            )
+    along = []
+    for d in turns:
+        mixed = weights[0] * y_s[d, e].astype(F32)
+        for j in range(1, n_ep):
+            across[d, j].wait()
+            mixed = mixed + weights[j] * y_r[d, j].astype(F32)
+        if d > 0:
+            m_s[d] = mixed.astype(BF16)
+            along.append(send(m_s.at[d], m_r.at[d], m_sem, d - 1, (e, at_z(d))))
     holder = t * share // feats
     slot = lax.rem(e + n_ep - holder, n_ep)
     start = pl.multiple_of(lax.rem(t * share, feats), share)
     total = res[slot, pl.ds(e * per, per), :, pl.ds(start, share)].astype(F32).reshape(seqs, share)
-    total = total + m_s[t].astype(F32)
-    for j in range(1, n_tp):
-        sent[j - 1].wait()
-        total = total + m_r[j].astype(F32)
+    total = total + mixed
+    for d in range(1, n_z):
+        along[d - 1].wait()
+        total = total + m_r[d].astype(F32)
     out[...] = total.astype(BF16)
+
+
+def finish(a, b, c, a_out, b_out, c_out):
+    a_out[...] = a[...]
+    b_out[...] = b[...]
+    c_out[...] = c[...]
 
 
 def body(
@@ -342,6 +405,7 @@
     tokens = seqs * n_ep
     rows = tokens // n_tp
     share = width // n_tp
+    n_z = n_tp // 2
     any_, vmem, smem = (
         pl.BlockSpec(memory_space=pl.ANY),
         pl.BlockSpec(memory_space=pltpu.VMEM),
@@ -352,13 +416,14 @@
     def like(a):
         return pltpu.VMEM(a.shape, a.dtype)
 
-    return pl.pallas_call(
+    shapes = (
+        jax.ShapeDtypeStruct((seqs, share), BF16),
+        jax.ShapeDtypeStruct((seqs, pc), BF16),
+        jax.ShapeDtypeStruct((seqs, pc), BF16),
+    )
+    results = pl.pallas_call(
         functools.partial(kernel, n_ep, n_tp),
-        out_shape=(
-            jax.ShapeDtypeStruct((seqs, share), BF16),
-            jax.ShapeDtypeStruct((seqs, pc), BF16),
-            jax.ShapeDtypeStruct((seqs, pc), BF16),
-        ),
+        out_shape=shapes,
         in_specs=[
             any_, vmem, any_, any_, any_, vmem, vmem, smem, any_, any_, smem, any_, vmem, vmem,
             vmem, any_, any_, any_,
@@ -377,8 +442,8 @@
             like(down_weight),
             pltpu.VMEM((n_ep, seqs, feats), BF16),
             pltpu.VMEM((n_ep, seqs // rows, rows, feats), F32),
-            pltpu.VMEM((n_ep, seqs, qc + 2 * pc), F32),
-            pltpu.VMEM((n_ep, seqs, qc + 2 * pc), F32),
+            pltpu.VMEM((n_ep, seqs, qc + 2 * pc), BF16),
+            pltpu.VMEM((n_ep, seqs, qc + 2 * pc), BF16),
             pltpu.VMEM((kv, seqs, lines, hd), F32),
             pltpu.VMEM((seqs, lines, cache), F32),
             pltpu.VMEM((seqs, lines, cache), F32),
@@ -387,19 +452,23 @@
             pltpu.VMEM((n_tp, rows, cols), BF16),
             pltpu.VMEM((n_tp, rows, cols), BF16),
             pltpu.VMEM((n_ep, n_tp, rows, cols), BF16),
-            pltpu.VMEM((n_ep, seqs, width), BF16),
-            pltpu.VMEM((n_ep, seqs, width), BF16),
-            pltpu.VMEM((n_tp, seqs, share), BF16),
-            pltpu.VMEM((n_tp, seqs, share), BF16),
+            pltpu.VMEM((n_z, n_ep, seqs, share), BF16),
+            pltpu.VMEM((n_z, n_ep, seqs, share), BF16),
+            pltpu.VMEM((n_z, n_ep, seqs, share), BF16),
+            pltpu.VMEM((n_z, n_ep, seqs, share), BF16),
+            pltpu.VMEM((n_z, seqs, share), BF16),
+            pltpu.VMEM((n_z, seqs, share), BF16),
             dma((11,)),
             dma((2, n_ep - 1)),
             dma((2, n_ep - 1)),
             dma((2, n_ep - 1)),
             dma((2, n_tp - 1)),
-            dma((2, n_tp - 1)),
-            dma((2, n_ep - 1)),
-            dma((2, n_ep - 1)),
-            dma((2, n_tp - 1)),
+            dma((2, n_z - 1)),
+            dma((2, n_z * (n_ep - 1))),
+            dma((2, n_z * n_ep)),
+            dma((2, n_z)),
+            dma((2, n_z * (n_ep - 1))),
+            dma((2, n_z - 1)),
         ],
         compiler_params=pltpu.CompilerParams(
             collective_id=0, has_side_effects=True, vmem_limit_bytes=60 * 2**20
@@ -418,12 +487,18 @@
         lengths,
         out_weight,
         expert_gain.reshape(1, -1),
-        routes,
-        route_weights,
+        routes.T,
+        route_weights.T,
         gate_weight,
         up_weight,
         down_weight,
     )
+    return pl.pallas_call(
+        finish,
+        out_shape=shapes,
+        in_specs=[vmem] * 3,
+        out_specs=(vmem,) * 3,
+    )(*results)
 
 
 def solution(mesh):

time: 58 us -> 46.5 us (0.80)
  local copies, waits for them, and re-layouts: 6.56 us -> 0 us
  Pallas kernels: 50.4 us -> 45.6 us
    unnamed x5 -> x0, local copies, waits for them, and re-layouts: 6.56 us -> none
    pallas_call x1 -> x2, Pallas kernels: 50.4 us -> 45.6 us  [the longest x1 44.3 us: body(): pl.pallas_call(functools.partial(kernel, n_ep, n_tp), out_shape=shapes, i...]
where the time goes in v2:
time: 46.5 us; the launch traced here: 46.3 us
  Pallas kernels  45.6 us (98%)
  between operations  0.65 us (1%)
    pallas_call x1, Pallas kernels, body(): pl.pallas_call(functools.partial(kernel, n_ep, n_tp), out_shape=shapes, i...  44.3 us
    pallas_call x1, Pallas kernels, body(): pl.pallas_call(finish, out_shape=shapes, in_specs=[vmem] * 3, out_specs=(...  1.34 us

profile of v2, /device:TPU:0, one launch (start us, length us, event | category | flops | bytes accessed | tf_op | source)
XLA Modules:
  0.0 46.3 jit_solution(5523916831996327612)
XLA Ops:
  0.6 44.3 %shard_map.193 = (bf16[16,512]{1,0:T(8,128)(2,1)}, bf16[16,128]{1,0:T(8,128)(2,1)}, bf16[16,128]{1,0:T(8,128)(2,1)}) custom-call(bf16[16,4096]{1,0:T(8,128)(2,1)} %hid.1, f32[1,4096]{1,0:T(1,128)} %bitcast.6, bf16[1024,512]{1,0:T(8,128)(2,1)} %wq_h.1, bf16[1024,128]{1,0:T(8,128)(2,1)} %wk_h.1, bf16[1024,128]{1,0:T(8,128)(2,1)} %wv_h.1, f32[1,128]{1,0:T(1,128)} %bitcast.10, ...), custom_call_target="tpu_custom_call" | custom-call | tf_op jit(solution)/shard_map/pallas_call | solution.py:424
  44.9 1.3 %shard_map.194 = (bf16[16,512]{1,0:T(8,128)(2,1)}, bf16[16,128]{1,0:T(8,128)(2,1)}, bf16[16,128]{1,0:T(8,128)(2,1)}) custom-call(bf16[16,512]{1,0:T(8,128)(2,1)} %get-tuple-element.6.a, bf16[16,128]{1,0:T(8,128)(2,1)} %get-tuple-element.7.b, bf16[16,128]{1,0:T(8,128)(2,1)} %get-tuple-element.8.c), custom_call_target="tpu_custom_call" | custom-call | tf_op jit(solution)/shard_map/pallas_call | solution.py:496

commit v3 on v2

--- a/solution.py
+++ b/solution.py
@@ -21,20 +21,20 @@
     n_ep,
     n_tp,
     hid,
-    attn_gain,
+    attn_gain_h,
     wq_h,
     wk_h,
     wv_h,
-    query_gain,
-    key_gain,
-    offset_s,
+    query_gain_h,
+    key_gain_h,
+    offset_h,
     kc_h,
     vc_h,
-    lengths_s,
+    lengths_h,
     wo_h,
-    expert_gain,
-    routes,
-    route_weights,
+    expert_gain_h,
+    routes_h,
+    route_weights_h,
     wg_h,
     wu_h,
     wd_h,
@@ -42,6 +42,14 @@
     fresh_k,
     fresh_v,
     hid_v,
+    attn_gain,
+    query_gain,
+    key_gain,
+    offset,
+    lengths,
+    expert_gain,
+    routes,
+    route_weights,
     wq,
     wk,
     wv,
@@ -121,8 +129,22 @@
         copy.start()
         return copy
 
+    barrier = pltpu.get_barrier_semaphore()
+    for j in range(1, n_ep):
+        pl.semaphore_signal(barrier, inc=1, device_id=(up_ep(j), t), device_id_type=MESH)
+    for j in range(1, n_tp):
+        pl.semaphore_signal(barrier, inc=1, device_id=(e, up_tp(j)), device_id_type=MESH)
+
     pairs = [
         (hid, hid_v),
+        (attn_gain_h, attn_gain),
+        (query_gain_h, query_gain),
+        (key_gain_h, key_gain),
+        (offset_h, offset),
+        (lengths_h, lengths),
+        (expert_gain_h, expert_gain),
+        (routes_h, routes),
+        (route_weights_h, route_weights),
         (hid.at[:, pl.ds(pl.multiple_of(e * feats, feats), feats)], xs.at[0]),
         (wq_h, wq),
         (wk_h, wk),
@@ -137,13 +159,10 @@
     copies = [pltpu.make_async_copy(a, b, local_sem.at[i]) for i, (a, b) in enumerate(pairs)]
     for copy in copies:
         copy.start()
-    c_hid, c_x0, c_q, c_k, c_v, c_kc, c_vc, c_wo, c_wg, c_wu, c_wd = copies
-
-    barrier = pltpu.get_barrier_semaphore()
-    for j in range(1, n_ep):
-        pl.semaphore_signal(barrier, inc=1, device_id=(up_ep(j), t), device_id_type=MESH)
-    for j in range(1, n_tp):
-        pl.semaphore_signal(barrier, inc=1, device_id=(e, up_tp(j)), device_id_type=MESH)
+    c_hid, *c_small, c_x0, c_q, c_k, c_v, c_kc, c_vc, c_wo, c_wg, c_wu, c_wd = copies
+
+    for copy in c_small:
+        copy.wait()
     weights = []
     same = lax.broadcasted_iota(jnp.int32, (seqs, seqs), 0) == lax.broadcasted_iota(
         jnp.int32, (seqs, seqs), 1
@@ -210,7 +229,7 @@
     for k in range(kv):
         shift = jnp.zeros((1, lines, 1), F32)
         for g in range(groups):
-            shift = jnp.where(line == g, offset_s[k * groups + g], shift)
+            shift = jnp.where(line == g, offset[:, k * groups + g : k * groups + g + 1][None], shift)
 
         def score(b, carry, k=k, shift=shift):
             qb = q_s[k, b].astype(BF16)
@@ -226,7 +245,7 @@
         lax.fori_loop(0, seqs, score, 0, unroll=True)
 
         limit = jnp.concatenate(
-            [jnp.full((1, lines, 1), lengths_s[b], jnp.int32) for b in range(seqs)], axis=0
+            [jnp.broadcast_to(lengths[:, b : b + 1][None], (1, lines, 1)) for b in range(seqs)], axis=0
         )
         carry = jnp.zeros((seqs * lines, 1), F32)
         for c in reversed(range(cache // span)):
@@ -284,7 +303,7 @@
         send(res.at[0, t], res.at[0, t], res_sem, d - 1, (e, at_z(d))) for d in range(1, n_z)
     ]
     across = {}
-    paired = []
+    paired = {}
     for d in range(n_z):
         if d > 0:
             along[d].wait()
@@ -297,22 +316,24 @@
                 d * (n_ep - 1) + j - 1,
                 (up_ep(j), t),
             )
-        paired.append(send(res.at[0, piece], res.at[0, piece], pair_sem, d, other))
-    for d in range(n_z):
-        piece = back_z(d)
-        for j in range(1, n_ep):
+        paired[d, 0] = send(res.at[0, piece], res.at[0, piece], pair_sem, d, other)
+    def forward(j):
+        for d in range(n_z):
+            piece = back_z(d)
             across[d, j].wait()
             at = d * (n_ep - 1) + j - 1 + n_z
-            paired.append(send(res.at[j, piece], res.at[j, piece], pair_sem, at, other))
+            paired[d, j] = send(res.at[j, piece], res.at[j, piece], pair_sem, at, other)
 
     c_wg.wait()
     c_wu.wait()
     square = jnp.zeros((tokens, 1), F32)
     gate = jnp.zeros((tokens, wg.shape[2]), F32)
     upward = jnp.zeros((tokens, wg.shape[2]), F32)
-    for copy in paired:
-        copy.wait()
     for j in range(n_ep):
+        if j + 1 < n_ep:
+            forward(j + 1)
+        for d in range(n_z):
+            paired[d, j].wait()
         at = pl.ds(pl.multiple_of(down_ep(j) * feats, feats), feats)
         r = res[j].astype(F32).reshape(tokens, feats)
         square = square + jnp.sum(r * r, axis=1, keepdims=True)
@@ -406,11 +427,8 @@
     rows = tokens // n_tp
     share = width // n_tp
     n_z = n_tp // 2
-    any_, vmem, smem = (
-        pl.BlockSpec(memory_space=pl.ANY),
-        pl.BlockSpec(memory_space=pltpu.VMEM),
-        pl.BlockSpec(memory_space=pltpu.SMEM),
-    )
+    any_ = pl.BlockSpec(memory_space=pl.ANY)
+    vmem = pl.BlockSpec(memory_space=pltpu.VMEM)
     dma = pltpu.SemaphoreType.DMA
 
     def like(a):
@@ -425,12 +443,19 @@
         functools.partial(kernel, n_ep, n_tp),
         out_shape=shapes,
         in_specs=[
-            any_, vmem, any_, any_, any_, vmem, vmem, smem, any_, any_, smem, any_, vmem, vmem,
-            vmem, any_, any_, any_,
-        ],
+            any_,
+        ] * 18,
         out_specs=(vmem, vmem, vmem),
         scratch_shapes=[
             like(hidden_in),
+            pltpu.VMEM((1, width), F32),
+            pltpu.VMEM((1, hd), F32),
+            pltpu.VMEM((1, hd), F32),
+            pltpu.VMEM((1, head_offset.shape[0]), F32),
+            pltpu.VMEM((1, seqs), jnp.int32),
+            pltpu.VMEM((1, width), F32),
+            pltpu.VMEM(routes.shape[::-1], jnp.int32),
+            pltpu.VMEM(routes.shape[::-1], F32),
             like(query_weight),
             like(key_weight),
             like(value_weight),
@@ -458,7 +483,7 @@
             pltpu.VMEM((n_z, n_ep, seqs, share), BF16),
             pltpu.VMEM((n_z, seqs, share), BF16),
             pltpu.VMEM((n_z, seqs, share), BF16),
-            dma((11,)),
+            dma((19,)),
             dma((2, n_ep - 1)),
             dma((2, n_ep - 1)),
             dma((2, n_ep - 1)),
@@ -481,10 +506,10 @@
         value_weight,
         query_gain.reshape(1, -1),
         key_gain.reshape(1, -1),
-        head_offset,
+        head_offset.reshape(1, -1),
         key_cache,
         value_cache,
-        lengths,
+        lengths.reshape(1, -1),
         out_weight,
         expert_gain.reshape(1, -1),
         routes.T,

time: 46.5 us -> 46 us (0.989)
  no operation moved by 1% of the time
where the time goes in v3:
time: 46 us; the launch traced here: 45.8 us
  Pallas kernels  45.2 us (98%)
  between operations  0.65 us (1%)
    pallas_call x1, Pallas kernels, body(): pl.pallas_call(functools.partial(kernel, n_ep, n_tp), out_shape=shapes, i...  43.8 us
    pallas_call x1, Pallas kernels, body(): pl.pallas_call(finish, out_shape=shapes, in_specs=[vmem] * 3, out_specs=(...  1.34 us

profile of v3, /device:TPU:0, one launch (start us, length us, event | category | flops | bytes accessed | tf_op | source)
XLA Modules:
  0.0 45.8 jit_solution(5276029118507106090)
XLA Ops:
  0.6 43.8 %shard_map.193 = (bf16[16,512]{1,0:T(8,128)(2,1)}, bf16[16,128]{1,0:T(8,128)(2,1)}, bf16[16,128]{1,0:T(8,128)(2,1)}) custom-call(bf16[16,4096]{1,0:T(8,128)(2,1)} %hid.1, f32[1,4096]{1,0:T(1,128)} %bitcast.8, bf16[1024,512]{1,0:T(8,128)(2,1)} %wq_h.1, bf16[1024,128]{1,0:T(8,128)(2,1)} %wk_h.1, bf16[1024,128]{1,0:T(8,128)(2,1)} %wv_h.1, f32[1,128]{1,0:T(1,128)} %bitcast.12, ...), custom_call_target="tpu_custom_call" | custom-call | tf_op jit(solution)/shard_map/pallas_call | solution.py:442
  44.5 1.3 %shard_map.194 = (bf16[16,512]{1,0:T(8,128)(2,1)}, bf16[16,128]{1,0:T(8,128)(2,1)}, bf16[16,128]{1,0:T(8,128)(2,1)}) custom-call(bf16[16,512]{1,0:T(8,128)(2,1)} %get-tuple-element.6.a, bf16[16,128]{1,0:T(8,128)(2,1)} %get-tuple-element.7.b, bf16[16,128]{1,0:T(8,128)(2,1)} %get-tuple-element.8.c), custom_call_target="tpu_custom_call" | custom-call | tf_op jit(solution)/shard_map/pallas_call | solution.py:521
